TPU v7x, 32 devices: a whole 2x2x4 slice. The times are simulated.
32 devices in a mesh: ep: 4 (over y, x), tp: 8 (over z, core).
Axes of the slice: x: 2, y: 2, z: 4, core: 2. Of those that a mesh axis runs over, the one named last changes fastest.
Arguments:
- queries: bfloat16 [4096, 1024], P('ep', 'tp'), may hold values from -6 to 6
- keys: bfloat16 [4096, 256], P('ep'), may hold values from -6 to 6, as said below
- values: bfloat16 [4096, 256], P('ep'), may hold values from -6 to 6
- slopes: float32 [16], P('tp'), may hold values from 0.002 to 0.08
- sinks: float32 [16], P('tp'), may hold values from 2 to 6
- out_weight: bfloat16 [1024, 2048], P('tp'), may hold values from -0.1875 to 0.1875
- mix_gain: float32 [2048], replicated, may hold values from 0.1 to 1.9
- moe_input: bfloat16 [4096, 2048], P(('ep', 'tp')), may hold values from -6 to 6
- in_gain: float32 [2048], replicated, may hold values from 0.1 to 1.9
- out_gain: float32 [2048], replicated, may hold values from 0.1 to 1.9
- group_router: bfloat16 [2048, 4], replicated, may hold values from -0.125 to 0.125
- expert_router: bfloat16 [2048, 4], replicated, may hold values from -0.125 to 0.125
- routes: int32 [4096, 2], P(('ep', 'tp')), may hold values from 0 to 3, all different within a row; in each aligned block of 128 rows (0 to 127, 128 to 255, ...) at most 96 rows name the same one
- gate_weight: bfloat16 [4, 2048, 1024], P('ep', None, 'tp'), may hold values from -0.125 to 0.125
- up_weight: bfloat16 [4, 2048, 1024], P('ep', None, 'tp'), may hold values from -0.125 to 0.125
- down_weight: bfloat16 [4, 2048, 1024], P('ep', None, 'tp'), may hold values from -0.1875 to 0.1875
Outputs:
- mixer_output: bfloat16 [4096, 2048], P(('ep', 'tp'))
- moe_output: bfloat16 [4096, 2048], P(('ep', 'tp'))
Inputs may be any that keep to these rules, and one draw needn't show every extreme that they name: `keys`: keys share one value range with the queries. `routes`: A token names 2 different experts. Among the rows of one device no expert is named more than 96 times, a bound that some block reaches in every draw.
All inputs are finite; a program needn't handle non-finite values.
Results may differ from a plain program's by a relative error of at most 0.018.
Values may be sent and summed in bfloat16 or wider, within the bound.
No kernel may reach another device: no remote copies, remote signals or barrier semaphores. Data moves between devices by JAX's collectives and lax.ppermute only.
A program may use at most 128 MiB of HBM per device.

v0:
```python
import math
import jax
import jax.numpy as jnp
from jax import lax
from jax.sharding import PartitionSpec as P

HEADS = 16
HD = 64
KV_HEADS = 4
WINDOW = 128
eps = 1e-06


def shifted(block, axis, distance):
    devices = range(lax.axis_size(axis))
    route = [(i - distance, i) for i in devices if i - distance in devices]
    return lax.ppermute(block, axis, route)


def scale_rows(matrix, gain):
    mean_square = jnp.mean(matrix * matrix, axis=-1, keepdims=True)
    return matrix * lax.rsqrt(mean_square + eps) * gain


def per_device(
    queries,
    keys,
    values,
    slopes,
    sinks,
    out_weight,
    mix_gain,
    moe_input,
    in_gain,
    out_gain,
    group_router,
    expert_router,
    routes,
    gate_weight,
    up_weight,
    down_weight,
):
    rows_group = queries.shape[0]
    local_heads = slopes.shape[0]
    per_kv = HEADS // KV_HEADS
    kv_index = lax.axis_index("tp") * local_heads // per_kv
    own_keys = lax.dynamic_slice_in_dim(keys, kv_index * HD, HD, 1)
    own_values = lax.dynamic_slice_in_dim(values, kv_index * HD, HD, 1)
    rim_keys, rim_values = shifted(
        (own_keys[rows_group - WINDOW :], own_values[rows_group - WINDOW :]), "ep", 1
    )
    blocks = rows_group // WINDOW
    key_blocks = own_keys.reshape(blocks, WINDOW, HD)
    value_blocks = own_values.reshape(blocks, WINDOW, HD)
    key_span = jnp.concatenate(
        [jnp.concatenate([rim_keys[None], key_blocks[:-1]], axis=0), key_blocks], axis=1
    )
    value_span = jnp.concatenate(
        [jnp.concatenate([rim_values[None], value_blocks[:-1]], axis=0), value_blocks], axis=1
    )
    query_blocks = queries.reshape(blocks, WINDOW, local_heads, HD)
    scores = jnp.einsum(
        "nqhd,nsd->nhqs", query_blocks, key_span, preferred_element_type=jnp.float32
    ) * (1.0 / math.sqrt(HD))
    query_index = jnp.arange(WINDOW, dtype=jnp.int32)[:, None]
    key_index = jnp.arange(2 * WINDOW, dtype=jnp.int32)[None, :]
    distance = query_index + WINDOW - key_index
    key_position = (
        lax.axis_index("ep") * rows_group
        + jnp.arange(blocks, dtype=jnp.int32)[:, None, None] * WINDOW
        + key_index[None]
        - WINDOW
    )
    valid = ((distance >= 0) & (distance < WINDOW))[None] & (key_position >= 0)
    scores = scores - slopes[None, :, None, None] * distance.astype(jnp.float32)[None, None]
    scores = jnp.where(valid[:, None], scores, -jnp.inf)
    sink = sinks[None, :, None, None]
    top = jnp.maximum(jnp.max(scores, axis=-1, keepdims=True), sink)
    weights = jnp.exp(scores - top)
    denom = jnp.sum(weights, axis=-1, keepdims=True) + jnp.exp(sink - top)
    probs = (weights / denom).astype(jnp.bfloat16)
    attention = jnp.einsum("nhqs,nsd->nqhd", probs, value_span, preferred_element_type=jnp.float32)
    attention = attention.astype(jnp.bfloat16).reshape(rows_group, local_heads * HD)
    own_rows = moe_input.shape[0]
    projected = lax.psum_scatter(
        jnp.dot(attention, out_weight, preferred_element_type=jnp.float32).astype(jnp.bfloat16),
        "tp",
        scatter_dimension=0,
        tiled=True,
    ).astype(jnp.float32)
    mixer_output = scale_rows(projected, mix_gain).astype(jnp.bfloat16)
    normed = scale_rows(moe_input.astype(jnp.float32), in_gain).astype(jnp.bfloat16)
    group_logits = jnp.dot(normed, group_router, preferred_element_type=jnp.float32)
    expert_logits = jnp.dot(normed, expert_router, preferred_element_type=jnp.float32)
    experts = expert_router.shape[1]
    groups = group_router.shape[1]
    per_group = experts // groups
    visits = routes.shape[1]
    expert_match = routes[:, :, None] == jnp.arange(experts, dtype=jnp.int32)[None, None, :]
    picked_logits = jnp.sum(jnp.where(expert_match, expert_logits[:, None, :], 0.0), axis=-1)
    group_prob = jax.nn.softmax(group_logits, axis=-1)
    group_match = (routes // per_group)[:, :, None] == jnp.arange(groups, dtype=jnp.int32)[
        None, None, :
    ]
    picked_group = jnp.sum(jnp.where(group_match, group_prob[:, None, :], 0.0), axis=-1)
    route_weight = picked_group * jax.nn.softmax(picked_logits, axis=-1)
    capacity = max(2, 3 * own_rows * visits // (2 * experts))
    match_int = expert_match.astype(jnp.int32).reshape(own_rows * visits, experts)
    before = jnp.cumsum(match_int, axis=0) - match_int
    slot = jnp.sum(before * match_int, axis=-1)
    position = (routes.reshape(-1) * capacity + slot).reshape(own_rows, visits)
    slot_ids = jnp.arange(experts * capacity, dtype=jnp.int32)
    placement = jnp.any(position[None, :, :] == slot_ids[:, None, None], axis=-1).astype(
        jnp.bfloat16
    )
    outgoing = jnp.dot(placement, normed, preferred_element_type=jnp.float32).astype(jnp.bfloat16)
    local_experts = gate_weight.shape[0]
    outgoing = outgoing.reshape(lax.axis_size("ep"), local_experts, capacity, normed.shape[1])
    arrived = lax.all_to_all(outgoing, "ep", split_axis=0, concat_axis=0, tiled=True)
    gate_piece = lax.all_gather(gate_weight, "tp", axis=2, tiled=True)
    up_piece = lax.all_gather(up_weight, "tp", axis=2, tiled=True)
    down_piece = lax.all_gather(down_weight, "tp", axis=2, tiled=True)
    gate = jnp.einsum("sxcd,xdf->sxcf", arrived, gate_piece, preferred_element_type=jnp.float32)
    up = jnp.einsum("sxcd,xdf->sxcf", arrived, up_piece, preferred_element_type=jnp.float32)
    hidden = (jax.nn.silu(gate) * up).astype(jnp.bfloat16)
    results = jnp.einsum("sxcf,xdf->sxcd", hidden, down_piece, preferred_element_type=jnp.float32)
    returned = lax.all_to_all(
        results.astype(jnp.bfloat16), "ep", split_axis=0, concat_axis=0, tiled=True
    )
    flat_back = returned.reshape(experts * capacity, returned.shape[3])
    picked_rows = jnp.take(flat_back, position.reshape(-1), axis=0).reshape(
        own_rows, visits, flat_back.shape[1]
    )
    moe = jnp.sum(route_weight[:, :, None] * picked_rows.astype(jnp.float32), axis=1)
    moe_output = scale_rows(moe, out_gain).astype(jnp.bfloat16)
    return (mixer_output, moe_output)


def solution(mesh):
    return jax.shard_map(
        per_device,
        mesh=mesh,
        in_specs=(
            P("ep", "tp"),
            P("ep", None),
            P("ep", None),
            P("tp"),
            P("tp"),
            P("tp", None),
            P(),
            P(("ep", "tp"), None),
            P(),
            P(),
            P(),
            P(),
            P(("ep", "tp"), None),
            P("ep", None, "tp"),
            P("ep", None, "tp"),
            P("ep", None, "tp"),
        ),
        out_specs=(P(("ep", "tp"), None), P(("ep", "tp"), None)),
        check_vma=False,
    )
```

profile of v0, /device:TPU:0, one launch (start us, length us, event | category | flops | bytes accessed | tf_op | source)
XLA Modules:
  0.0 222.8 jit_solution(3067624268574023449)
XLA Ops:
  7.2 0.0 copy-start
  7.2 0.0 all-gather.6.cloned.1.call-start
  7.2 0.7 all-gather.6.cloned.1.call-update
  7.9 0.0 all-gather.4.cloned.1.call-start
  8.0 0.7 all-gather.4.cloned.1.call-update
  8.7 0.0 all-gather.8.cloned.1.call-start
  8.7 0.7 all-gather.8.cloned.1.call-update
  9.4 0.0 reduce-scatter.2.cloned.1.call-start
  9.5 1.2 constant_dynamic-slice_fusion
  10.7 0.1 copy.112
  10.9 4.9 %collective-permute-start.1 = (bf16[128,64]{0,1:T(8,128)(2,1)S(1)}, bf16[128,64]{0,1:T(8,128)(2,1)S(1)}, u32[]{:S(2)}, u32[]{:S(2)}) collective-permute-start(bf16[128,64]{0,1:T(8,128)(2,1)S(1)} %slice.36), channel_id=1, source_target_pairs={{0,8},{8,16},{16,24},{1,9},{9,17},{17,25},{2,10},{10,18},{18,26},{... | collective-permute-start | bytes 49160 | tf_op jit(solution)/shard_map/ppermute | solution.py:17
  15.8 0.1 copy.111
  15.9 3.4 %collective-permute-start = (bf16[128,64]{0,1:T(8,128)(2,1)S(1)}, bf16[128,64]{0,1:T(8,128)(2,1)S(1)}, u32[]{:S(2)}, u32[]{:S(2)}) collective-permute-start(bf16[128,64]{0,1:T(8,128)(2,1)S(1)} %slice.34), channel_id=1, source_target_pairs={{0,8},{8,16},{16,24},{1,9},{9,17},{17,25},{2,10},{10,18},{18,26},{... | collective-permute-start | bytes 49160 | tf_op jit(solution)/shard_map/ppermute | solution.py:17
  19.3 0.1 add_compare_fusion
  19.6 0.3 broadcast_and_fusion
  19.9 0.1 broadcast_multiply_fusion
  20.1 0.2 reshape.313
  20.3 0.0 copy-start.7
  20.3 0.6 fusion.73
  21.0 0.0 copy-done.7
  21.0 0.1 broadcast_maximum_fusion
  21.1 0.3 fusion.13
  21.4 0.1 exponential_add_fusion
  21.5 0.0 collective-permute-done
  21.5 0.5 fusion.20
  22.0 0.2 copy.95
  22.2 3.2 %convolution_convert_fusion = bf16[1024,2048]{1,0:T(8,128)(2,1)} fusion(bf16[128,2048]{1,0:T(8,128)(2,1)S(1)} %copy-done, bf16[16,8,8,128]{3,2,1,0:T(8,128)(2,1)S(1)} %bitcast.155), kind=kOutput, calls=%fused_computation.7 | convolution fusion | flops 538968064 | bytes 4980736 | tf_op jit(solution)/shard_map/dot_general | solution.py:86
  25.4 0.0 reduce-scatter.2.cloned.1.call-update
  25.4 0.6 copy-done.3
  26.1 0.1 copy.97
  26.2 0.1 eq.56
  26.3 0.1 reshape.291
  26.5 1.2 reduce-window.6
  27.7 0.1 slice.38
  27.8 0.1 copy.99
  27.9 0.1 copy.100
  28.0 0.1 add_bitcast_fusion
  28.1 0.1 reduce_sum.102
  28.3 0.1 copy.101
  28.4 0.2 fusion.33
  28.6 1.8 convolution_convert_fusion.1
  30.4 3.9 %all-to-all-start = ((bf16[4,1,96,2048]{3,2,1,0:T(8,128)(2,1)}), bf16[4,1,96,2048]{3,2,1,0:T(8,128)(2,1)S(1)}, u32[]{:S(2)}, u32[]{:S(2)}) async-start(bf16[4,1,96,2048]{3,2,1,0:T(8,128)(2,1)} %bitcast.11), calls=%async_computation.1 | async-start | bytes 3145728 | tf_op jit(solution)/shard_map/all_to_all | solution.py:119
  34.3 0.3 fusion.74
  34.7 0.3 fusion.68
  35.1 0.1 copy.96
  35.2 0.1 copy.105
  35.3 0.1 mul.175
  35.5 17.6 %all-to-all-done = bf16[4,1,96,2048]{3,2,1,0:T(8,128)(2,1)S(1)} async-done(((bf16[4,1,96,2048]{3,2,1,0:T(8,128)(2,1)}), bf16[4,1,96,2048]{3,2,1,0:T(8,128)(2,1)S(1)}, u32[]{:S(2)}, u32[]{:S(2)}) %all-to-all-start) | async-done | bytes 1572896 | tf_op jit(solution)/shard_map/all_to_all | solution.py:119
  53.1 7.1 %all-gather.6.cloned.1.call-done = bf16[1,2048,1024]{2,1,0:T(8,128)(2,1)} async-done(((bf16[1,2048,128]{2,1,0:T(8,128)(2,1)}), bf16[1,2048,1024]{2,1,0:T(8,128)(2,1)}) %all-gather.6.cloned.1.call-update) | async-done | bytes 4194320 | tf_op jit(solution)/shard_map/all_gather | solution.py:121
  60.2 5.1 %fusion.2 = f32[4,96,1024]{2,1,0:T(8,128)} fusion(bf16[1,2048,1024]{2,1,0:T(8,128)(2,1)} %all-gather.6.cloned.1.call-done, bf16[4,1,96,2048]{3,2,1,0:T(8,128)(2,1)S(1)} %all-to-all-done), kind=kOutput, calls=%fused_computation.3 | convolution fusion | flops 1610612736 | bytes 7340032 | tf_op jit(solution)/shard_map/sxcd,xdf->sxcf/dot_general | solution.py:124
  65.3 42.5 %all-gather.4.cloned.1.call-done = bf16[1,2048,1024]{2,1,0:T(8,128)(2,1)} async-done(((bf16[1,2048,128]{2,1,0:T(8,128)(2,1)}), bf16[1,2048,1024]{2,1,0:T(8,128)(2,1)}) %all-gather.4.cloned.1.call-update) | async-done | bytes 4194320 | tf_op jit(solution)/shard_map/all_gather | solution.py:120
  107.8 47.6 %all-gather.8.cloned.1.call-done = bf16[1,2048,1024]{2,1,0:T(8,128)(2,1)} async-done(((bf16[1,2048,128]{2,1,0:T(8,128)(2,1)}), bf16[1,2048,1024]{2,1,0:T(8,128)(2,1)}) %all-gather.8.cloned.1.call-update) | async-done | bytes 4194320 | tf_op jit(solution)/shard_map/all_gather | solution.py:122
  155.4 8.6 %fusion.9 = bf16[4,1,96,2048]{3,2,1,0:T(8,128)(2,1)} fusion(bf16[1,2048,1024]{2,1,0:T(8,128)(2,1)} %all-gather.8.cloned.1.call-done, f32[4,96,1024]{2,1,0:T(8,128)} %fusion.2, bf16[1,2048,1024]{2,1,0:T(8,128)(2,1)} %all-gather.4.cloned.1.call-done, bf16[4,1,96,2048]{3,2,1,0:T(8,128)(2,1)S(1)} %all-to-all-done), kind=kOutput, calls=%fused_computation.10 | convolution fusion | flops 3224371200 | bytes 13107200 | tf_op jit(solution)/shard_map/sxcf,xdf->sxcd/dot_general | solution.py:126
  164.1 3.9 %all-to-all-start.1 = ((bf16[4,1,96,2048]{3,2,1,0:T(8,128)(2,1)}), bf16[4,1,96,2048]{3,2,1,0:T(8,128)(2,1)S(1)}, u32[]{:S(2)}, u32[]{:S(2)}) async-start(bf16[4,1,96,2048]{3,2,1,0:T(8,128)(2,1)} %fusion.9), calls=%async_computation.2 | async-start | bytes 3145728 | tf_op jit(solution)/shard_map/all_to_all | solution.py:127
  167.9 0.1 copy.102
  168.1 37.6 %reduce-scatter.2.cloned.1.call-done = bf16[128,2048]{1,0:T(8,128)(2,1)} async-done(((bf16[1024,2048]{1,0:T(8,128)(2,1)}), bf16[128,2048]{1,0:T(8,128)(2,1)}) %reduce-scatter.2.cloned.1.call-update) | async-done | bytes 524304 | tf_op jit(solution)/shard_map/reduce_scatter | solution.py:85
  205.7 1.2 fusion.30
  207.0 2.0 fusion.32
  209.0 1.4 gather_fusion
  210.4 0.7 gather.7
  211.1 0.0 copy-start.6
  211.1 4.1 %multiply_reduce_fusion = f32[128,2048]{1,0:T(8,128)S(1)} fusion(bf16[128,2,2048]{2,1,0:T(2,128)(2,1)S(1)} %gather.7, pred[128,2]{1,0:T(8,128)(4,1)S(1)} %copy.102, f32[128,2]{1,0:T(8,128)S(1)} %copy.96), kind=kLoop, calls=%fused_computation.13 | loop fusion | flops 1835008 | bytes 2098432 | tf_op jit(solution)/shard_map/reduce_sum | solution.py:134
  215.2 0.2 multiply_reduce_fusion.1
  215.3 1.0 multiply_convert_fusion
  (47 shorter events, 0.5 us)
Async XLA Ops:
  7.2 15.0 %copy-start = (bf16[128,2048]{1,0:T(8,128)(2,1)S(1)}, bf16[128,2048]{1,0:T(8,128)(2,1)}, u32[]{:S(2)}) copy-start(bf16[128,2048]{1,0:T(8,128)(2,1)} %param.21) | copy-start | bytes 1572868
  7.2 53.0 %all-gather.6.cloned.1.call-start = ((), (), s32[]{:S(2)}) async-start(), calls=%async_computation.5 | async-start | bytes 4718592 | tf_op jit(solution)/shard_map/all_gather | solution.py:121
  7.9 12.0 %copy-start.8 = (f32[2]{0:T(128)S(1)}, f32[2]{0:T(128)}, u32[]{:S(2)}) copy-start(f32[2]{0:T(128)} %param.19) | copy-start | bytes 28
  7.9 99.9 %all-gather.4.cloned.1.call-start = ((), (), s32[]{:S(2)}) async-start(), calls=%async_computation.4 | async-start | bytes 4718592 | tf_op jit(solution)/shard_map/all_gather | solution.py:120
  8.7 11.4 %copy-start.2 = (bf16[1024,128]{1,0:T(8,128)(2,1)S(1)}, bf16[1024,128]{1,0:T(8,128)(2,1)}, u32[]{:S(2)}) copy-start(bf16[1024,128]{1,0:T(8,128)(2,1)} %param.16) | copy-start | bytes 786436
  8.7 146.7 %all-gather.8.cloned.1.call-start = ((), (), s32[]{:S(2)}) async-start(), calls=%async_computation.6 | async-start | bytes 4718592 | tf_op jit(solution)/shard_map/all_gather | solution.py:122
  9.4 196.3 %reduce-scatter.2.cloned.1.call-start = ((), (), s32[]{:S(2)}) async-start(), calls=%async_computation.3 | async-start | bytes 4718592 | tf_op jit(solution)/shard_map/reduce_scatter | solution.py:85
  10.9 9.4 %collective-permute-start.1 = (bf16[128,64]{0,1:T(8,128)(2,1)S(1)}, bf16[128,64]{0,1:T(8,128)(2,1)S(1)}, u32[]{:S(2)}, u32[]{:S(2)}) collective-permute-start(bf16[128,64]{0,1:T(8,128)(2,1)S(1)} %slice.36), channel_id=1, source_target_pairs={{0,8},{8,16},{16,24},{1,9},{9,17},{17,25},{2,10},{10,18},{18,26},{... | collective-permute-start | bytes 49160 | tf_op jit(solution)/shard_map/ppermute | solution.py:17
  15.9 5.6 %collective-permute-start = (bf16[128,64]{0,1:T(8,128)(2,1)S(1)}, bf16[128,64]{0,1:T(8,128)(2,1)S(1)}, u32[]{:S(2)}, u32[]{:S(2)}) collective-permute-start(bf16[128,64]{0,1:T(8,128)(2,1)S(1)} %slice.34), channel_id=1, source_target_pairs={{0,8},{8,16},{16,24},{1,9},{9,17},{17,25},{2,10},{10,18},{18,26},{... | collective-permute-start | bytes 49160 | tf_op jit(solution)/shard_map/ppermute | solution.py:17
  20.3 0.7 copy-start.7
  25.4 0.7 copy-start.3
  25.4 3.0 %copy-start.1 = (bf16[128,2048]{1,0:T(8,128)(2,1)S(1)}, bf16[128,2048]{1,0:T(8,128)(2,1)}, u32[]{:S(2)}) copy-start(bf16[128,2048]{1,0:T(8,128)(2,1)} %param.23) | copy-start | bytes 1572868
  25.4 3.2 %copy-start.4 = (f32[2048]{0:T(1024)S(1)}, f32[2048]{0:T(1024)}, u32[]{:S(2)}) copy-start(f32[2048]{0:T(1024)} %param.24) | copy-start | bytes 24580
  30.4 3.9 %copy-start.9 = (bf16[2048,4]{0,1:T(4,128)(2,1)S(1)}, bf16[2048,4]{0,1:T(4,128)(2,1)}, u32[]{:S(2)}) copy-start(bf16[2048,4]{0,1:T(4,128)(2,1)} %param.26) | copy-start | bytes 49156
  30.4 4.3 %copy-start.10 = (bf16[2048,4]{0,1:T(4,128)(2,1)S(1)}, bf16[2048,4]{0,1:T(4,128)(2,1)}, u32[]{:S(2)}) copy-start(bf16[2048,4]{0,1:T(4,128)(2,1)} %param.27) | copy-start | bytes 49156
  30.4 22.6 %all-to-all-start = ((bf16[4,1,96,2048]{3,2,1,0:T(8,128)(2,1)}), bf16[4,1,96,2048]{3,2,1,0:T(8,128)(2,1)S(1)}, u32[]{:S(2)}, u32[]{:S(2)}) async-start(bf16[4,1,96,2048]{3,2,1,0:T(8,128)(2,1)} %bitcast.11), calls=%async_computation.1 | async-start | bytes 3145728 | tf_op jit(solution)/shard_map/all_to_all | solution.py:119
  164.1 42.9 %copy-start.5 = (f32[2048]{0:T(1024)S(1)}, f32[2048]{0:T(1024)}, u32[]{:S(2)}) copy-start(f32[2048]{0:T(1024)} %param.22) | copy-start | bytes 24580
  164.1 44.9 %all-to-all-start.1 = ((bf16[4,1,96,2048]{3,2,1,0:T(8,128)(2,1)}), bf16[4,1,96,2048]{3,2,1,0:T(8,128)(2,1)S(1)}, u32[]{:S(2)}, u32[]{:S(2)}) async-start(bf16[4,1,96,2048]{3,2,1,0:T(8,128)(2,1)} %fusion.9), calls=%async_computation.2 | async-start | bytes 3145728 | tf_op jit(solution)/shard_map/all_to_all | solution.py:127
  211.1 4.3 %copy-start.6 = (f32[2048]{0:T(1024)S(1)}, f32[2048]{0:T(1024)}, u32[]{:S(2)}) copy-start(f32[2048]{0:T(1024)} %param.25) | copy-start | bytes 24580
Sparse Core Ops, SparseCore 0:
  9.6 50.5 all-gather.5
  61.7 45.9 all-gather.3
  109.4 45.9 all-gather.7
  157.6 48.1 reduce-scatter.1
where the time goes:
time: 223 us
  waiting for transfers between devices  155 us (70%)
  matrix products  20.5 us (9%)
  starting transfers between devices  16.2 us (7%)
  between operations  14.2 us (6%)
  other arithmetic  11.3 us (5%)
  local copies, waits for them, and re-layouts  6.18 us (3%)
    all_gather x1, waiting for transfers between devices, per_device(): down_piece = lax.all_gather(down_weight, 'tp', axis=2, tiled=True)  47.6 us
    all_gather x1, waiting for transfers between devices, per_device(): gate_piece = lax.all_gather(gate_weight, 'tp', axis=2, tiled=True)  42.5 us
    reduce_scatter x1, waiting for transfers between devices, per_device(): lax.psum_scatter(jnp.dot(attention, out_weight, preferred_element_type=jn...  37.6 us
    all_to_all x1, waiting for transfers between devices, per_device(): lax.all_to_all(outgoing, 'ep', split_axis=0, concat_axis=0, tiled=True)  17.6 us
    dot_general x1, matrix products, per_device(): jnp.einsum('sxcf,xdf->sxcd', hidden, down_piece, preferred_element_type=j...  8.63 us
    ppermute x2, starting transfers between devices, shifted(): return lax.ppermute(block, axis, route)  8.27 us
    all_gather x1, waiting for transfers between devices, per_device(): up_piece = lax.all_gather(up_weight, 'tp', axis=2, tiled=True)  7.09 us
    dot_general x1, matrix products, per_device(): jnp.einsum('sxcd,xdf->sxcf', arrived, up_piece, preferred_element_type=jn...  5.13 us
  transfers between devices with their start and end apart: 8, of which 5 were waited for; matrix products, arithmetic and copies ran while one was open for 13% of the time, Pallas kernels for 0%

commit v1 on v0

--- a/solution.py
+++ b/solution.py
@@ -117,7 +117,16 @@
     local_experts = gate_weight.shape[0]
     outgoing = outgoing.reshape(lax.axis_size("ep"), local_experts, capacity, normed.shape[1])
     arrived = lax.all_to_all(outgoing, "ep", split_axis=0, concat_axis=0, tiled=True)
-    gate_piece = lax.all_gather(gate_weight, "tp", axis=2, tiled=True)
+    ways = lax.axis_size("tp")
+    up_2 = [(d, (d + 1) % ways) for d in range(ways)]
+    down = [(d, (d - 1) % ways) for d in range(ways)]
+    earlier, later = ([gate_weight], [gate_weight])
+    for _ in range(ways // 2):
+        earlier.append(lax.ppermute(earlier[-1], "tp", up_2))
+    for _ in range((ways - 1) // 2):
+        later.append(lax.ppermute(later[-1], "tp", down))
+    line = jnp.concatenate([*earlier[::-1], *later[1:]], axis=2)
+    gate_piece = jnp.roll(line, (lax.axis_index("tp") - ways // 2) * gate_weight.shape[2], axis=2)
     up_piece = lax.all_gather(up_weight, "tp", axis=2, tiled=True)
     down_piece = lax.all_gather(down_weight, "tp", axis=2, tiled=True)
     gate = jnp.einsum("sxcd,xdf->sxcf", arrived, gate_piece, preferred_element_type=jnp.float32)

time: 223 us -> 199 us (0.89)
  waiting for transfers between devices: 155 us -> 97.5 us
  local copies, waits for them, and re-layouts: 6.18 us -> 25.5 us
  starting transfers between devices: 16.2 us -> 29.4 us
    all_gather x1 -> x0, waiting for transfers between devices: 42.5 us -> none  [per_device(): gate_piece = lax.all_gather(gate_weight, 'tp', axis=2, tiled=True)]
    ppermute x0 -> x7, waiting for transfers between devices: none -> 33.8 us  [the longest x4 33.7 us: per_device(): earlier.append(lax.ppermute(earlier[-1], 'tp', up_2))]
    all_gather x1, waiting for transfers between devices: 47.6 us -> 24.4 us  [per_device(): down_piece = lax.all_gather(down_weight, 'tp', axis=2, tiled=True)]
    unnamed x25 -> x42, local copies, waits for them, and re-layouts: 1.09 us -> 19.6 us
    all_to_all x1, waiting for transfers between devices: 17.6 us -> 0.01 us  [per_device(): lax.all_to_all(outgoing, 'ep', split_axis=0, concat_axis=0, tiled=True)]
    ppermute x0 -> x7, starting transfers between devices: none -> 13.8 us  [the longest x3 11.3 us: per_device(): later.append(lax.ppermute(later[-1], 'tp', down))]
    all_gather x1, waiting for transfers between devices: 7.09 us -> 0.01 us  [per_device(): up_piece = lax.all_gather(up_weight, 'tp', axis=2, tiled=True)]
  transfers between devices with their start and end apart: 8 -> 14, of which waited for: 5 -> 6; matrix products, arithmetic and copies ran while one was open for 13% -> 25% of each run, Pallas kernels for 0% -> 0%
where the time goes in v1:
time: 199 us; the launch traced here: 198 us
  waiting for transfers between devices  97.5 us (49%)
  starting transfers between devices  29.4 us (15%)
  local copies, waits for them, and re-layouts  25.5 us (13%)
  matrix products  20.1 us (10%)
  between operations  14.2 us (7%)
  other arithmetic  11.2 us (6%)
    reduce_scatter x1, waiting for transfers between devices, per_device(): lax.psum_scatter(jnp.dot(attention, out_weight, preferred_element_type=jn...  38 us
    ppermute x4, waiting for transfers between devices, per_device(): earlier.append(lax.ppermute(earlier[-1], 'tp', up_2))  33.7 us
    all_gather x1, waiting for transfers between devices, per_device(): down_piece = lax.all_gather(down_weight, 'tp', axis=2, tiled=True)  24.4 us
    unnamed x42, local copies, waits for them, and re-layouts  19.6 us
    ppermute x3, starting transfers between devices, per_device(): later.append(lax.ppermute(later[-1], 'tp', down))  11.3 us
    dot_general x1, matrix products, per_device(): jnp.einsum('sxcf,xdf->sxcd', hidden, down_piece, preferred_element_type=j...  8.67 us
    ppermute x2, starting transfers between devices, shifted(): return lax.ppermute(block, axis, route)  7.23 us
    dot_general x1, matrix products, per_device(): jnp.einsum('sxcd,xdf->sxcf', arrived, up_piece, preferred_element_type=jn...  4.56 us
  transfers between devices with their start and end apart: 14, of which 6 were waited for; matrix products, arithmetic and copies ran while one was open for 25% of the time, Pallas kernels for 0%

profile of v1, /device:TPU:0, one launch (start us, length us, event | category | flops | bytes accessed | tf_op | source)
XLA Modules:
  0.0 197.9 jit_solution(2270993233735532060)
XLA Ops:
  7.2 0.7 all-gather.3.cloned.1.call-update
  8.0 0.7 all-gather.5.cloned.1.call-update
  8.7 0.5 collective-permute-start.2
  9.3 4.1 %collective-permute-start.6 = (bf16[1,2048,128]{2,1,0:T(8,128)(2,1)}, bf16[1,2048,128]{2,1,0:T(8,128)(2,1)S(1)}, u32[]{:S(2)}, u32[]{:S(2)}) collective-permute-start(bf16[1,2048,128]{2,1,0:T(8,128)(2,1)} %param.29), channel_id=1, source_target_pairs={{0,7},{1,0},{2,1},{3,2},{4,3},{5,4},{6,5},{7,6},{8,15},{9,8},{10,9... | collective-permute-start | bytes 1572872 | tf_op jit(solution)/shard_map/ppermute | solution.py:127
  13.4 1.2 constant_dynamic-slice_fusion
  14.6 0.1 copy.112
  14.8 3.8 %collective-permute-start.1 = (bf16[128,64]{0,1:T(8,128)(2,1)S(1)}, bf16[128,64]{0,1:T(8,128)(2,1)S(1)}, u32[]{:S(2)}, u32[]{:S(2)}) collective-permute-start(bf16[128,64]{0,1:T(8,128)(2,1)S(1)} %slice.36), channel_id=1, source_target_pairs={{0,8},{8,16},{16,24},{1,9},{9,17},{17,25},{2,10},{10,18},{18,26},{... | collective-permute-start | bytes 49160 | tf_op jit(solution)/shard_map/ppermute | solution.py:17
  18.6 0.1 copy.111
  18.8 3.4 %collective-permute-start = (bf16[128,64]{0,1:T(8,128)(2,1)S(1)}, bf16[128,64]{0,1:T(8,128)(2,1)S(1)}, u32[]{:S(2)}, u32[]{:S(2)}) collective-permute-start(bf16[128,64]{0,1:T(8,128)(2,1)S(1)} %slice.34), channel_id=1, source_target_pairs={{0,8},{8,16},{16,24},{1,9},{9,17},{17,25},{2,10},{10,18},{18,26},{... | collective-permute-start | bytes 49160 | tf_op jit(solution)/shard_map/ppermute | solution.py:17
  22.2 0.8 copy.97
  23.0 0.1 eq.59
  23.1 1.2 reduce-window.6
  24.9 0.3 broadcast_and_fusion
  25.4 0.1 reshape.291
  25.6 0.2 reshape.313
  25.9 0.6 fusion.76
  26.6 0.3 fusion.14
  27.0 0.5 fusion.30
  27.5 0.2 copy.95
  27.7 3.3 %convolution_convert_fusion = bf16[1024,2048]{1,0:T(8,128)(2,1)} fusion(bf16[128,2048]{1,0:T(8,128)(2,1)S(1)} %copy-done, bf16[16,8,8,128]{3,2,1,0:T(8,128)(2,1)S(1)} %bitcast.153), kind=kOutput, calls=%fused_computation.8 | convolution fusion | flops 538968064 | bytes 4980736 | tf_op jit(solution)/shard_map/dot_general | solution.py:86
  31.0 0.1 reduce_sum.102
  31.2 0.8 copy-done.1
  32.0 0.2 fusion.34
  32.3 1.8 convolution_convert_fusion.1
  34.2 4.5 %all-to-all-start = ((bf16[4,1,96,2048]{3,2,1,0:T(8,128)(2,1)}), bf16[4,1,96,2048]{3,2,1,0:T(8,128)(2,1)}, u32[]{:S(2)}, u32[]{:S(2)}) async-start(bf16[4,1,96,2048]{3,2,1,0:T(8,128)(2,1)} %bitcast.13), calls=%async_computation.1 | async-start | bytes 3145728 | tf_op jit(solution)/shard_map/all_to_all | solution.py:119
  38.7 0.3 fusion.77
  39.0 10.4 %collective-permute-done.3 = bf16[1,2048,128]{2,1,0:T(8,128)(2,1)S(1)} collective-permute-done((bf16[1,2048,128]{2,1,0:T(8,128)(2,1)S(1)}, bf16[1,2048,128]{2,1,0:T(8,128)(2,1)S(1)}, u32[]{:S(2)}, u32[]{:S(2)}) %collective-permute-start.3) | collective-permute-done | bytes 524320 | tf_op jit(solution)/shard_map/ppermute | solution.py:125
  49.4 0.3 fusion.71
  49.8 3.5 %collective-permute-start.7 = (bf16[1,2048,128]{2,1,0:T(8,128)(2,1)S(1)}, bf16[1,2048,128]{2,1,0:T(8,128)(2,1)S(1)}, u32[]{:S(2)}, u32[]{:S(2)}) collective-permute-start(bf16[1,2048,128]{2,1,0:T(8,128)(2,1)S(1)} %collective-permute-done.6), channel_id=1, source_target_pairs={{0,7},{1,0},{2,1},{3,2},{4,3},{5,4},{6,5},{7,6},{8,15},{9,8},{10,9... | collective-permute-start | bytes 1572872 | tf_op jit(solution)/shard_map/ppermute | solution.py:127
  53.3 18.6 %collective-permute-done.4 = bf16[1,2048,128]{2,1,0:T(8,128)(2,1)} collective-permute-done((bf16[1,2048,128]{2,1,0:T(8,128)(2,1)S(1)}, bf16[1,2048,128]{2,1,0:T(8,128)(2,1)}, u32[]{:S(2)}, u32[]{:S(2)}) %collective-permute-start.4) | collective-permute-done | bytes 524320 | tf_op jit(solution)/shard_map/ppermute | solution.py:125
  71.9 1.9 collective-permute-start.5
  73.8 0.1 copy.105
  73.9 0.1 mul.179
  74.3 3.7 %collective-permute-start.8 = (bf16[1,2048,128]{2,1,0:T(8,128)(2,1)S(1)}, bf16[1,2048,128]{2,1,0:T(8,128)(2,1)S(1)}, u32[]{:S(2)}, u32[]{:S(2)}) collective-permute-start(bf16[1,2048,128]{2,1,0:T(8,128)(2,1)S(1)} %collective-permute-done.7), channel_id=1, source_target_pairs={{0,7},{1,0},{2,1},{3,2},{4,3},{5,4},{6,5},{7,6},{8,15},{9,8},{10,9... | collective-permute-start | bytes 1572872 | tf_op jit(solution)/shard_map/ppermute | solution.py:127
  78.1 4.7 %collective-permute-done.5 = bf16[1,2048,128]{2,1,0:T(8,128)(2,1)} collective-permute-done((bf16[1,2048,128]{2,1,0:T(8,128)(2,1)}, bf16[1,2048,128]{2,1,0:T(8,128)(2,1)}, u32[]{:S(2)}, u32[]{:S(2)}) %collective-permute-start.5) | collective-permute-done | bytes 524320 | tf_op jit(solution)/shard_map/ppermute | solution.py:125
  82.7 2.0 constant_dynamic-update-slice_fusion.15
  84.7 2.0 %constant_dynamic-update-slice_fusion.14 = bf16[1,2048,2048]{2,1,0:T(8,128)(2,1)} fusion(bf16[1,2048,2048]{2,1,0:T(8,128)(2,1)} %constant_dynamic-update-slice_fusion.15, bf16[1,2048,128]{2,1,0:T(8,128)(2,1)} %collective-permute-done.4), kind=kLoop, calls=%fused_computation.86 | loop fusion | bytes 1048576
  86.7 0.9 constant_dynamic-update-slice_fusion.13
  87.6 0.9 constant_dynamic-update-slice_fusion.12
  88.4 0.9 constant_dynamic-update-slice_fusion.11
  89.3 0.9 constant_dynamic-update-slice_fusion.10
  90.2 0.9 constant_dynamic-update-slice_fusion.9
  91.1 0.9 constant_dynamic-update-slice_fusion.8
  92.0 1.9 constant_dynamic-update-slice_fusion.7
  94.0 2.0 constant_dynamic-update-slice_fusion.6
  95.9 0.9 constant_dynamic-update-slice_fusion.5
  96.8 0.9 constant_dynamic-update-slice_fusion.4
  97.7 0.9 constant_dynamic-update-slice_fusion.3
  98.6 0.9 constant_dynamic-update-slice_fusion.2
  99.6 0.9 constant_dynamic-update-slice_fusion.1
  100.4 0.9 constant_dynamic-update-slice_fusion
  101.3 4.6 %fusion.2 = f32[4,96,1024]{2,1,0:T(8,128)S(1)} fusion(bf16[1,2048,1024]{2,1,0:T(8,128)(2,1)} %all-gather.3.cloned.1.call-done, bf16[4,1,96,2048]{3,2,1,0:T(8,128)(2,1)} %all-to-all-done), kind=kOutput, calls=%fused_computation.3 | convolution fusion | flops 1610612736 | bytes 7340032 | tf_op jit(solution)/shard_map/sxcd,xdf->sxcf/dot_general | solution.py:133
  105.9 24.4 %all-gather.5.cloned.1.call-done = bf16[1,2048,1024]{2,1,0:T(8,128)(2,1)} async-done(((bf16[1,2048,128]{2,1,0:T(8,128)(2,1)}), bf16[1,2048,1024]{2,1,0:T(8,128)(2,1)}) %all-gather.5.cloned.1.call-update) | async-done | bytes 4194320 | tf_op jit(solution)/shard_map/all_gather | solution.py:131
  130.3 8.7 %fusion.10 = bf16[4,1,96,2048]{3,2,1,0:T(8,128)(2,1)} fusion(bf16[1,2048,1024]{2,1,0:T(8,128)(2,1)} %all-gather.5.cloned.1.call-done, f32[4,96,1024]{2,1,0:T(8,128)S(1)} %fusion.2, bf16[4,1,96,2048]{3,2,1,0:T(8,128)(2,1)} %all-to-all-done, bf16[1,2048,2048]{2,1,0:T(8,128)(2,1)} %constant_dynamic-update-slice_fusion, s32[]{:T(128)S(6)} %select_n.64), kind=kOutput, calls=%fused_computation.11 | convolution fusion | flops 3224371200 | bytes 13107204 | tf_op jit(solution)/shard_map/sxcf,xdf->sxcd/dot_general | solution.py:135
  138.9 3.8 %all-to-all-start.1 = ((bf16[4,1,96,2048]{3,2,1,0:T(8,128)(2,1)}), bf16[4,1,96,2048]{3,2,1,0:T(8,128)(2,1)S(1)}, u32[]{:S(2)}, u32[]{:S(2)}) async-start(bf16[4,1,96,2048]{3,2,1,0:T(8,128)(2,1)} %fusion.10), calls=%async_computation.2 | async-start | bytes 3145728 | tf_op jit(solution)/shard_map/all_to_all | solution.py:136
  142.7 0.1 copy.102
  142.9 38.0 %reduce-scatter.2.cloned.1.call-done = bf16[128,2048]{1,0:T(8,128)(2,1)} async-done(((bf16[1024,2048]{1,0:T(8,128)(2,1)}), bf16[128,2048]{1,0:T(8,128)(2,1)}) %reduce-scatter.2.cloned.1.call-update) | async-done | bytes 524304 | tf_op jit(solution)/shard_map/reduce_scatter | solution.py:85
  180.8 1.2 fusion.31
  182.1 2.0 %fusion.33 = bf16[128,2048]{1,0:T(8,128)(2,1)} fusion(bf16[128,2048]{1,0:T(8,128)(2,1)} %reduce-scatter.2.cloned.1.call-done, f32[2048]{0:T(1024)S(1)} %copy-done.6, f32[128]{0:T(128)S(1)} %add_rsqrt_fusion.2), kind=kLoop, calls=%fused_computation.37 | loop fusion | flops 1048576 | bytes 1057280 | tf_op jit(solution)/shard_map/convert_element_type | solution.py:91
  184.1 1.4 gather_fusion
  185.5 0.7 gather.7
  186.2 4.1 %multiply_reduce_fusion = f32[128,2048]{1,0:T(8,128)S(1)} fusion(bf16[128,2,2048]{2,1,0:T(2,128)(2,1)S(1)} %gather.7, pred[128,2]{1,0:T(8,128)(4,1)S(1)} %copy.102, f32[128,2]{1,0:T(8,128)S(1)} %copy.96), kind=kLoop, calls=%fused_computation.14 | loop fusion | flops 1835008 | bytes 2098432 | tf_op jit(solution)/shard_map/reduce_sum | solution.py:143
  190.3 0.2 multiply_reduce_fusion.1
  190.5 1.0 multiply_convert_fusion
  (76 shorter events, 1.6 us)
Async XLA Ops:
  7.2 20.5 %copy-start = (bf16[128,2048]{1,0:T(8,128)(2,1)S(1)}, bf16[128,2048]{1,0:T(8,128)(2,1)}, u32[]{:S(2)}) copy-start(bf16[128,2048]{1,0:T(8,128)(2,1)} %param.21) | copy-start | bytes 1572868
  7.2 18.1 %copy-start.9 = (f32[2]{0:T(128)S(1)}, f32[2]{0:T(128)}, u32[]{:S(2)}) copy-start(f32[2]{0:T(128)} %param.19) | copy-start | bytes 28
  7.2 18.4 %copy-start.3 = (bf16[1024,128]{1,0:T(8,128)(2,1)S(1)}, bf16[1024,128]{1,0:T(8,128)(2,1)}, u32[]{:S(2)}) copy-start(bf16[1024,128]{1,0:T(8,128)(2,1)} %param.16) | copy-start | bytes 786436
  7.2 94.1 %all-gather.3.cloned.1.call-start = ((), (), s32[]{:S(2)}) async-start(), calls=%async_computation.4 | async-start | bytes 4718592 | tf_op jit(solution)/shard_map/all_gather | solution.py:130
  7.9 122.3 %all-gather.5.cloned.1.call-start = ((), (), s32[]{:S(2)}) async-start(), calls=%async_computation.5 | async-start | bytes 4718592 | tf_op jit(solution)/shard_map/all_gather | solution.py:131
  8.7 172.1 %reduce-scatter.2.cloned.1.call-start = ((), (), s32[]{:S(2)}) async-start(), calls=%async_computation.3 | async-start | bytes 4718592 | tf_op jit(solution)/shard_map/reduce_scatter | solution.py:85
  8.7 23.5 %collective-permute-start.2 = (bf16[1,2048,128]{2,1,0:T(8,128)(2,1)}, bf16[1,2048,128]{2,1,0:T(8,128)(2,1)S(1)}, u32[]{:S(2)}, u32[]{:S(2)}) collective-permute-start(bf16[1,2048,128]{2,1,0:T(8,128)(2,1)} %param.29), channel_id=1, source_target_pairs={{0,1},{1,2},{2,3},{3,4},{4,5},{5,6},{6,7},{7,0},{8,9},{9,10},{10,1... | collective-permute-start | bytes 1572872 | tf_op jit(solution)/shard_map/ppermute | solution.py:125
  9.3 40.5 %collective-permute-start.6 = (bf16[1,2048,128]{2,1,0:T(8,128)(2,1)}, bf16[1,2048,128]{2,1,0:T(8,128)(2,1)S(1)}, u32[]{:S(2)}, u32[]{:S(2)}) collective-permute-start(bf16[1,2048,128]{2,1,0:T(8,128)(2,1)} %param.29), channel_id=1, source_target_pairs={{0,7},{1,0},{2,1},{3,2},{4,3},{5,4},{6,5},{7,6},{8,15},{9,8},{10,9... | collective-permute-start | bytes 1572872 | tf_op jit(solution)/shard_map/ppermute | solution.py:127
  14.6 11.9 %copy-start.8 = (f32[2]{0:T(128)S(1)}, f32[2]{0:T(128)}, u32[]{:S(2)}) copy-start(f32[2]{0:T(128)} %param.20) | copy-start | bytes 28
  14.8 11.1 %collective-permute-start.1 = (bf16[128,64]{0,1:T(8,128)(2,1)S(1)}, bf16[128,64]{0,1:T(8,128)(2,1)S(1)}, u32[]{:S(2)}, u32[]{:S(2)}) collective-permute-start(bf16[128,64]{0,1:T(8,128)(2,1)S(1)} %slice.36), channel_id=1, source_target_pairs={{0,8},{8,16},{16,24},{1,9},{9,17},{17,25},{2,10},{10,18},{18,26},{... | collective-permute-start | bytes 49160 | tf_op jit(solution)/shard_map/ppermute | solution.py:17
  18.8 8.2 %collective-permute-start = (bf16[128,64]{0,1:T(8,128)(2,1)S(1)}, bf16[128,64]{0,1:T(8,128)(2,1)S(1)}, u32[]{:S(2)}, u32[]{:S(2)}) collective-permute-start(bf16[128,64]{0,1:T(8,128)(2,1)S(1)} %slice.34), channel_id=1, source_target_pairs={{0,8},{8,16},{16,24},{1,9},{9,17},{17,25},{2,10},{10,18},{18,26},{... | collective-permute-start | bytes 49160 | tf_op jit(solution)/shard_map/ppermute | solution.py:17
  30.9 1.0 copy-start.1
  30.9 1.2 copy-start.4
  30.9 1.4 copy-start.5
  30.9 7.7 %copy-start.10 = (bf16[2048,4]{0,1:T(4,128)(2,1)S(1)}, bf16[2048,4]{0,1:T(4,128)(2,1)}, u32[]{:S(2)}) copy-start(bf16[2048,4]{0,1:T(4,128)(2,1)} %param.26) | copy-start | bytes 49156
  31.0 18.5 %copy-start.11 = (bf16[2048,4]{0,1:T(4,128)(2,1)S(1)}, bf16[2048,4]{0,1:T(4,128)(2,1)}, u32[]{:S(2)}) copy-start(bf16[2048,4]{0,1:T(4,128)(2,1)} %param.27) | copy-start | bytes 49156
  32.2 17.2 %collective-permute-start.3 = (bf16[1,2048,128]{2,1,0:T(8,128)(2,1)S(1)}, bf16[1,2048,128]{2,1,0:T(8,128)(2,1)S(1)}, u32[]{:S(2)}, u32[]{:S(2)}) collective-permute-start(bf16[1,2048,128]{2,1,0:T(8,128)(2,1)S(1)} %collective-permute-done.2), channel_id=1, source_target_pairs={{0,1},{1,2},{2,3},{3,4},{4,5},{5,6},{6,7},{7,0},{8,9},{9,10},{10,1... | collective-permute-start | bytes 1572872 | tf_op jit(solution)/shard_map/ppermute | solution.py:125
  34.2 54.3 %copy-start.2 = (bf16[1,2048,128]{2,1,0:T(8,128)(2,1)S(1)}, bf16[1,2048,128]{2,1,0:T(8,128)(2,1)}, u32[]{:S(2)}) copy-start(bf16[1,2048,128]{2,1,0:T(8,128)(2,1)} %param.29) | copy-start | bytes 1572868
  34.2 67.1 %all-to-all-start = ((bf16[4,1,96,2048]{3,2,1,0:T(8,128)(2,1)}), bf16[4,1,96,2048]{3,2,1,0:T(8,128)(2,1)}, u32[]{:S(2)}, u32[]{:S(2)}) async-start(bf16[4,1,96,2048]{3,2,1,0:T(8,128)(2,1)} %bitcast.13), calls=%async_computation.1 | async-start | bytes 3145728 | tf_op jit(solution)/shard_map/all_to_all | solution.py:119
  49.4 22.5 %collective-permute-start.4 = (bf16[1,2048,128]{2,1,0:T(8,128)(2,1)S(1)}, bf16[1,2048,128]{2,1,0:T(8,128)(2,1)}, u32[]{:S(2)}, u32[]{:S(2)}) collective-permute-start(bf16[1,2048,128]{2,1,0:T(8,128)(2,1)S(1)} %collective-permute-done.3), channel_id=1, source_target_pairs={{0,1},{1,2},{2,3},{3,4},{4,5},{5,6},{6,7},{7,0},{8,9},{9,10},{10,1... | collective-permute-start | bytes 1572872 | tf_op jit(solution)/shard_map/ppermute | solution.py:125
  49.8 24.6 %collective-permute-start.7 = (bf16[1,2048,128]{2,1,0:T(8,128)(2,1)S(1)}, bf16[1,2048,128]{2,1,0:T(8,128)(2,1)S(1)}, u32[]{:S(2)}, u32[]{:S(2)}) collective-permute-start(bf16[1,2048,128]{2,1,0:T(8,128)(2,1)S(1)} %collective-permute-done.6), channel_id=1, source_target_pairs={{0,7},{1,0},{2,1},{3,2},{4,3},{5,4},{6,5},{7,6},{8,15},{9,8},{10,9... | collective-permute-start | bytes 1572872 | tf_op jit(solution)/shard_map/ppermute | solution.py:127
  71.9 10.8 %collective-permute-start.5 = (bf16[1,2048,128]{2,1,0:T(8,128)(2,1)}, bf16[1,2048,128]{2,1,0:T(8,128)(2,1)}, u32[]{:S(2)}, u32[]{:S(2)}) collective-permute-start(bf16[1,2048,128]{2,1,0:T(8,128)(2,1)} %collective-permute-done.4), channel_id=1, source_target_pairs={{0,1},{1,2},{2,3},{3,4},{4,5},{5,6},{6,7},{7,0},{8,9},{9,10},{10,1... | collective-permute-start | bytes 1572872 | tf_op jit(solution)/shard_map/ppermute | solution.py:125
  74.3 16.8 %collective-permute-start.8 = (bf16[1,2048,128]{2,1,0:T(8,128)(2,1)S(1)}, bf16[1,2048,128]{2,1,0:T(8,128)(2,1)S(1)}, u32[]{:S(2)}, u32[]{:S(2)}) collective-permute-start(bf16[1,2048,128]{2,1,0:T(8,128)(2,1)S(1)} %collective-permute-done.7), channel_id=1, source_target_pairs={{0,7},{1,0},{2,1},{3,2},{4,3},{5,4},{6,5},{7,6},{8,15},{9,8},{10,9... | collective-permute-start | bytes 1572872 | tf_op jit(solution)/shard_map/ppermute | solution.py:127
  105.9 76.2 %copy-start.6 = (f32[2048]{0:T(1024)S(1)}, f32[2048]{0:T(1024)}, u32[]{:S(2)}) copy-start(f32[2048]{0:T(1024)} %param.22) | copy-start | bytes 24580
  138.9 45.2 %all-to-all-start.1 = ((bf16[4,1,96,2048]{3,2,1,0:T(8,128)(2,1)}), bf16[4,1,96,2048]{3,2,1,0:T(8,128)(2,1)S(1)}, u32[]{:S(2)}, u32[]{:S(2)}) async-start(bf16[4,1,96,2048]{3,2,1,0:T(8,128)(2,1)} %fusion.10), calls=%async_computation.2 | async-start | bytes 3145728 | tf_op jit(solution)/shard_map/all_to_all | solution.py:136
  185.5 5.0 %copy-start.7 = (f32[2048]{0:T(1024)S(1)}, f32[2048]{0:T(1024)}, u32[]{:S(2)}) copy-start(f32[2048]{0:T(1024)} %param.25) | copy-start | bytes 24580
Sparse Core Ops, SparseCore 0:
  9.6 65.6 all-gather.2
  76.8 53.3 all-gather.4
  132.6 48.2 reduce-scatter.1
